TPU v7x, 32 devices: a whole 2x2x4 slice. The times are simulated.
32 devices in a mesh: fs: 4 (over z), rep: 4 (over y, x), tp: 2 (over core).
Axes of the slice: x: 2, y: 2, z: 4, core: 2. Of those that a mesh axis runs over, the one named last changes fastest.
Arguments:
- normed_input: bfloat16 [2048, 1024], P(('fs', 'rep')), may hold values from -6 to 6
- query_cotangent: bfloat16 [2048, 512], P(('fs', 'rep'), 'tp'), may hold values from -0.029907227 to 0.029907227
- value_cotangent: bfloat16 [2048, 1024], P(('fs', 'rep'), 'tp'), may hold values from -0.029907227 to 0.029907227
- query_basis: bfloat16 [1024, 128], replicated, may hold values from -0.1875 to 0.1875
- value_basis: bfloat16 [1024, 128], replicated, may hold values from -0.1875 to 0.1875
- query_weight: float32 [1024, 512], P(('fs', 'rep'), 'tp'), may hold values from -0.1875 to 0.1875
- value_weight: float32 [1024, 1024], P(('fs', 'rep'), 'tp'), may hold values from -0.1875 to 0.1875
- query_first: float32 [128, 512], P(('fs', 'rep'), 'tp'), may hold values from -6 to 6
- query_second: float32 [128, 512], P(('fs', 'rep'), 'tp'), may hold values from 0.25 to 4
- value_first: float32 [128, 1024], P(('fs', 'rep'), 'tp'), may hold values from -6 to 6
- value_second: float32 [128, 1024], P(('fs', 'rep'), 'tp'), may hold values from 0.25 to 4
Outputs:
- query_update: float32 [1024, 512], P(('fs', 'rep'), 'tp')
- value_update: float32 [1024, 1024], P(('fs', 'rep'), 'tp')
- query_weight_new: float32 [1024, 512], P(('fs', 'rep'), 'tp')
- value_weight_new: float32 [1024, 1024], P(('fs', 'rep'), 'tp')
- query_first_new: float32 [128, 512], P(('fs', 'rep'), 'tp')
- query_second_new: float32 [128, 512], P(('fs', 'rep'), 'tp')
- value_first_new: float32 [128, 1024], P(('fs', 'rep'), 'tp')
- value_second_new: float32 [128, 1024], P(('fs', 'rep'), 'tp')
- query_copy: bfloat16 [1024, 512], P(None, 'tp')
- value_copy: bfloat16 [1024, 1024], P(None, 'tp')
All inputs are finite; a program needn't handle non-finite values.
Results may differ from a plain program's by a relative error of at most 0.001.
Values may be sent and summed in bfloat16 or wider, within the bound.
A program may use at most 64 MiB of HBM per device.

v0:
```python
import jax
import jax.numpy as jnp
from jax import lax
from jax.sharding import PartitionSpec as P


def moments(projected, first_old, second_old):
    first_new = 0.9 * first_old + 0.1 * projected
    second_new = 0.99 * second_old + 0.01 * projected * projected
    return (first_new, second_new, first_new / (jnp.sqrt(second_new) + 1e-08))


def finish(whole_dir, basis_rows, weight, squares, entries):
    norm_scale = jnp.sqrt(squares / entries + 1.0)
    update = jnp.dot(basis_rows, whole_dir, precision=lax.Precision.HIGHEST) / norm_scale
    weight_new = weight - 0.01 * update
    return (update, weight_new, weight_new.astype(jnp.bfloat16))


def split_parts(reduced):
    high_part = reduced.astype(jnp.bfloat16)
    held = lax.optimization_barrier(high_part)
    low_part = (reduced - held.astype(jnp.float32)).astype(jnp.bfloat16)
    return (high_part, low_part)


def parts_product(high_part, low_part, cotangent):
    dims = (((0,), (0,)), ((), ()))
    first_term = lax.dot_general(high_part, cotangent, dims, preferred_element_type=jnp.float32)
    second_term = lax.dot_general(low_part, cotangent, dims, preferred_element_type=jnp.float32)
    return first_term + second_term


def body(
    normed_input,
    query_cotangent,
    value_cotangent,
    query_basis,
    value_basis,
    query_weight,
    value_weight,
    query_first,
    query_second,
    value_first,
    value_second,
):
    row_count = query_weight.shape[0]
    query_width = query_cotangent.shape[1]
    offset = lax.axis_index(("fs", "rep")) * row_count
    query_rows = lax.dynamic_slice_in_dim(query_basis, offset, row_count, 0).astype(jnp.float32)
    value_rows = lax.dynamic_slice_in_dim(value_basis, offset, row_count, 0).astype(jnp.float32)
    reduced_query = jnp.dot(normed_input, query_basis, preferred_element_type=jnp.float32)
    reduced_value = jnp.dot(normed_input, value_basis, preferred_element_type=jnp.float32)
    query_high, query_low = split_parts(reduced_query)
    value_high, value_low = split_parts(reduced_value)
    projected = lax.psum_scatter(
        jnp.concatenate(
            [
                parts_product(query_high, query_low, query_cotangent),
                parts_product(value_high, value_low, value_cotangent),
            ],
            axis=1,
        ),
        ("fs", "rep"),
        scatter_dimension=0,
        tiled=True,
    )
    query_projected = projected[:, :query_width]
    value_projected = projected[:, query_width:]
    query_first_new, query_second_new, query_dir = moments(
        query_projected, query_first, query_second
    )
    value_first_new, value_second_new, value_dir = moments(
        value_projected, value_first, value_second
    )
    query_whole, value_whole = (
        lax.all_gather(query_dir, ("fs", "rep"), axis=0, tiled=True),
        lax.all_gather(value_dir, ("fs", "rep"), axis=0, tiled=True),
    )
    query_squares, value_squares = lax.psum(
        (jnp.sum(query_dir * query_dir), jnp.sum(value_dir * value_dir)), ("fs", "rep", "tp")
    )
    tp_count = lax.axis_size("tp")
    query_update, query_weight_new, query_half = finish(
        query_whole,
        query_rows,
        query_weight,
        query_squares,
        query_whole.shape[0] * query_whole.shape[1] * tp_count,
    )
    value_update, value_weight_new, value_half = finish(
        value_whole,
        value_rows,
        value_weight,
        value_squares,
        value_whole.shape[0] * value_whole.shape[1] * tp_count,
    )
    query_copy, value_copy = (
        lax.all_gather(query_half, ("fs", "rep"), axis=0, tiled=True),
        lax.all_gather(value_half, ("fs", "rep"), axis=0, tiled=True),
    )
    return (
        query_update,
        value_update,
        query_weight_new,
        value_weight_new,
        query_first_new,
        query_second_new,
        value_first_new,
        value_second_new,
        query_copy,
        value_copy,
    )


def solution(mesh):
    in_specs = (
        P(("fs", "rep"), None),
        P(("fs", "rep"), "tp"),
        P(("fs", "rep"), "tp"),
        P(),
        P(),
        P(("fs", "rep"), "tp"),
        P(("fs", "rep"), "tp"),
        P(("fs", "rep"), "tp"),
        P(("fs", "rep"), "tp"),
        P(("fs", "rep"), "tp"),
        P(("fs", "rep"), "tp"),
    )
    out_specs = (
        P(("fs", "rep"), "tp"),
        P(("fs", "rep"), "tp"),
        P(("fs", "rep"), "tp"),
        P(("fs", "rep"), "tp"),
        P(("fs", "rep"), "tp"),
        P(("fs", "rep"), "tp"),
        P(("fs", "rep"), "tp"),
        P(("fs", "rep"), "tp"),
        P(None, "tp"),
        P(None, "tp"),
    )
    return jax.shard_map(body, mesh=mesh, in_specs=in_specs, out_specs=out_specs, check_vma=False)
```

profile of v0, /device:TPU:0, one launch (start us, length us, event | category | flops | bytes accessed | tf_op | source)
XLA Modules:
  0.0 313.8 jit_solution(15066968954675229272)
XLA Ops:
  7.2 0.0 copy-start
  7.2 0.0 copy-start.3
  7.2 0.0 reduce-scatter.2.cloned.1.call-start
  7.2 0.9 copy-done
  8.1 0.0 copy-start.4
  8.1 1.2 fusion.10
  9.3 0.0 copy-start.2
  9.4 0.0 copy-done.3
  9.4 0.2 fusion.13
  9.6 0.0 copy-done.4
  9.6 0.7 copy-done.2
  10.3 0.0 copy-start.5
  10.3 0.2 fusion.11
  10.5 0.6 copy-done.5
  11.1 0.2 fusion.12
  11.3 0.2 convolution_add_fusion
  11.6 0.2 convolution_add_fusion.1
  11.8 0.8 pad_maximum_fusion
  12.5 0.0 copy-start.9
  12.5 0.0 reduce-scatter.2.cloned.1.call-update
  12.6 0.0 copy-start.8
  12.6 0.0 all-gather.2.cloned.1.call-start
  12.6 0.0 copy-start.10
  12.6 0.0 copy-start.11
  12.7 126.3 %reduce-scatter.2.cloned.1.call-done = f32[8,768]{1,0:T(8,128)} async-done(((f32[128,768]{1,0:T(8,128)}), f32[8,768]{1,0:T(8,128)}) %reduce-scatter.2.cloned.1.call-update) | async-done | bytes 24592 | tf_op jit(solution)/shard_map/reduce_scatter | solution.py:56
  138.9 0.0 copy-done.9
  138.9 0.0 copy-done.8
  138.9 1.9 multiply_reduce_fusion
  140.9 0.0 copy-done.10
  140.9 0.0 copy-done.11
  140.9 1.9 multiply_reduce_fusion.1
  142.8 40.4 %all-reduce = (f32[]{:T(128)}, f32[]{:T(128)}) all-reduce(f32[]{:T(128)} %get-tuple-element.20, f32[]{:T(128)} %get-tuple-element.16), channel_id=1, replica_groups=mesh['fs'=4,'rep'=4,'tp'=2] {'fs','rep','tp'}, use_global_device_ids=true, to_apply=%region_2.0 | all-reduce | flops 2 | bytes 16 | tf_op jit(solution)/shard_map/psum | solution.py:80
  183.9 0.0 copy-start.6
  183.9 40.3 %all_gather.13 = f32[128,512]{1,0:T(8,128)S(1)} all-gather(f32[8,512]{1,0:T(8,128)S(1)} %get-tuple-element.17), channel_id=1, replica_groups=mesh['fs'=4,'rep'=4,'tp'=2] {'fs','rep'}, dimensions={0}, use_global_device_ids=true | all-gather | bytes 278528 | tf_op jit(solution)/shard_map/all_gather | solution.py:78
  224.2 0.0 copy-done.6
  224.2 1.0 fusion.6
  225.2 0.0 all-gather.2.cloned.1.call-update
  225.9 0.0 copy-start.7
  225.9 36.5 %all_gather.12 = f32[128,256]{1,0:T(8,128)S(1)} all-gather(f32[8,256]{1,0:T(8,128)S(1)} %get-tuple-element.21), channel_id=1, replica_groups=mesh['fs'=4,'rep'=4,'tp'=2] {'fs','rep'}, dimensions={0}, use_global_device_ids=true | all-gather | bytes 139264 | tf_op jit(solution)/shard_map/all_gather | solution.py:77
  262.3 0.0 copy-done.7
  262.3 0.8 fusion.7
  263.2 41.4 %all_gather.14 = bf16[1024,256]{1,0:T(8,128)(2,1)S(1)} all-gather(bf16[64,256]{1,0:T(8,128)(2,1)S(1)} %get-tuple-element.14), channel_id=1, replica_groups=mesh['fs'=4,'rep'=4,'tp'=2] {'fs','rep'}, dimensions={0}, use_global_device_ids=true | all-gather | bytes 557056 | tf_op jit(solution)/shard_map/all_gather | solution.py:99
  304.5 0.0 all-gather.2.cloned.1.call-done
  304.5 0.0 copy-start.1
  304.5 0.8 copy.23
  305.3 0.6 copy-done.1
  306.0 1.0 copy.24
Async XLA Ops:
  7.2 1.0 copy-start
  7.2 2.2 copy-start.3
  7.2 131.7 %reduce-scatter.2.cloned.1.call-start = ((), (), s32[]{:S(2)}) async-start(), calls=%async_computation.1 | async-start | bytes 417792 | tf_op jit(solution)/shard_map/reduce_scatter | solution.py:56
  8.1 1.5 copy-start.4
  9.3 1.0 copy-start.2
  10.3 0.8 copy-start.5
  12.5 126.4 %copy-start.9 = (f32[8,512]{1,0:T(8,128)S(1)}, f32[8,512]{1,0:T(8,128)}, u32[]{:S(2)}) copy-start(f32[8,512]{1,0:T(8,128)} %param.20) | copy-start | bytes 49156
  12.6 126.4 %copy-start.8 = (f32[8,512]{1,0:T(8,128)S(1)}, f32[8,512]{1,0:T(8,128)}, u32[]{:S(2)}) copy-start(f32[8,512]{1,0:T(8,128)} %param.21) | copy-start | bytes 49156
  12.6 292.0 %all-gather.2.cloned.1.call-start = ((), (), s32[]{:S(2)}) async-start(), calls=%async_computation.2 | async-start | bytes 1114112 | tf_op jit(solution)/shard_map/all_gather | solution.py:100
  12.6 128.2 %copy-start.10 = (f32[8,256]{1,0:T(8,128)S(1)}, f32[8,256]{1,0:T(8,128)}, u32[]{:S(2)}) copy-start(f32[8,256]{1,0:T(8,128)} %param.19) | copy-start | bytes 24580
  12.6 128.2 %copy-start.11 = (f32[8,256]{1,0:T(8,128)S(1)}, f32[8,256]{1,0:T(8,128)}, u32[]{:S(2)}) copy-start(f32[8,256]{1,0:T(8,128)} %param.18) | copy-start | bytes 24580
  183.9 40.3 %copy-start.6 = (f32[64,512]{1,0:T(8,128)S(1)}, f32[64,512]{1,0:T(8,128)}, u32[]{:S(2)}) copy-start(f32[64,512]{1,0:T(8,128)} %param.17) | copy-start | bytes 393220
  225.9 36.5 %copy-start.7 = (f32[64,256]{1,0:T(8,128)S(1)}, f32[64,256]{1,0:T(8,128)}, u32[]{:S(2)}) copy-start(f32[64,256]{1,0:T(8,128)} %param.16) | copy-start | bytes 196612
  304.5 1.4 copy-start.1
Sparse Core Ops, SparseCore 0:
  13.2 125.6 reduce-scatter.1
  225.3 52.1 all-gather.1
where the time goes:
time: 314 us
  blocking collectives  159 us (51%)
  waiting for transfers between devices  126 us (40%)
  between operations  15.6 us (5%)
  local copies, waits for them, and re-layouts  4.65 us (1%)
  other arithmetic  4.61 us (1%)
  matrix products  4.03 us (1%)
    reduce_scatter x1, waiting for transfers between devices, body(): lax.psum_scatter(jnp.concatenate([parts_product(query_high, query_low, qu...  126 us
    all_gather x1, blocking collectives, body(): lax.all_gather(query_half, ('fs', 'rep'), axis=0, tiled=True)  41.4 us
    psum x1, blocking collectives, body(): lax.psum((jnp.sum(query_dir * query_dir), jnp.sum(value_dir * value_dir))...  40.4 us
    all_gather x1, blocking collectives, body(): lax.all_gather(value_dir, ('fs', 'rep'), axis=0, tiled=True)  40.3 us
    all_gather x1, blocking collectives, body(): lax.all_gather(query_dir, ('fs', 'rep'), axis=0, tiled=True)  36.5 us
  transfers between devices with their start and end apart: 2, of which 1 were waited for; matrix products, arithmetic and copies ran while one was open for 0% of the time, Pallas kernels for 0%

commit v1 on v0

--- a/solution.py
+++ b/solution.py
@@ -74,7 +74,12 @@
         value_projected, value_first, value_second
     )
     query_whole, value_whole = (
-        lax.all_gather(query_dir, ("fs", "rep"), axis=0, tiled=True),
+        jnp.concatenate(
+            lax.all_to_all(
+                jnp.stack([query_dir] * lax.axis_size(("fs", "rep"))), ("fs", "rep"), 0, 0
+            ),
+            axis=0,
+        ),
         lax.all_gather(value_dir, ("fs", "rep"), axis=0, tiled=True),
     )
     query_squares, value_squares = lax.psum(

time: 314 us -> 289 us (0.920)
  blocking collectives: 159 us -> 122 us
  waiting for transfers between devices: 126 us -> 134 us
  starting transfers between devices: 0.08 us -> 3.72 us
    all_gather x1 -> x0, blocking collectives: 36.5 us -> none  [body(): lax.all_gather(query_dir, ('fs', 'rep'), axis=0, tiled=True)]
    all_to_all x0 -> x1, waiting for transfers between devices: none -> 7.27 us  [body(): lax.all_to_all(jnp.stack([query_dir] * lax.axis_size(('fs', 'rep'))), ('f...]
    all_to_all x0 -> x1, starting transfers between devices: none -> 3.64 us  [body(): lax.all_to_all(jnp.stack([query_dir] * lax.axis_size(('fs', 'rep'))), ('f...]
  transfers between devices with their start and end apart: 2 -> 3, of which waited for: 1 -> 2; matrix products, arithmetic and copies ran while one was open for 0% -> 1% of each run, Pallas kernels for 0% -> 0%
where the time goes in v1:
time: 289 us
  waiting for transfers between devices  134 us (46%)
  blocking collectives  122 us (42%)
  between operations  15.6 us (5%)
  local copies, waits for them, and re-layouts  5.31 us (2%)
  other arithmetic  4.61 us (2%)
  matrix products  4.03 us (1%)
  starting transfers between devices  3.72 us (1%)
    reduce_scatter x1, waiting for transfers between devices, body(): lax.psum_scatter(jnp.concatenate([parts_product(query_high, query_low, qu...  126 us
    all_gather x1, blocking collectives, body(): lax.all_gather(query_half, ('fs', 'rep'), axis=0, tiled=True)  41.1 us
    psum x1, blocking collectives, body(): lax.psum((jnp.sum(query_dir * query_dir), jnp.sum(value_dir * value_dir))...  40.4 us
    all_gather x1, blocking collectives, body(): lax.all_gather(value_dir, ('fs', 'rep'), axis=0, tiled=True)  40.3 us
    all_to_all x1, waiting for transfers between devices, body(): lax.all_to_all(jnp.stack([query_dir] * lax.axis_size(('fs', 'rep'))), ('f...  7.27 us
  transfers between devices with their start and end apart: 3, of which 2 were waited for; matrix products, arithmetic and copies ran while one was open for 1% of the time, Pallas kernels for 0%

profile of v1, /device:TPU:0, one launch (start us, length us, event | category | flops | bytes accessed | tf_op | source)
XLA Modules:
  0.0 288.6 jit_solution(9641706617914831413)
XLA Ops:
  7.2 0.0 copy-start
  7.2 0.0 copy-start.3
  7.2 0.0 reduce-scatter.2.cloned.1.call-start
  7.2 0.9 copy-done
  8.1 0.0 copy-start.4
  8.1 1.2 fusion.11
  9.3 0.0 copy-start.2
  9.4 0.0 copy-done.3
  9.4 0.2 fusion.14
  9.6 0.0 copy-done.4
  9.6 0.7 copy-done.2
  10.3 0.0 copy-start.5
  10.3 0.2 fusion.12
  10.5 0.6 copy-done.5
  11.1 0.2 fusion.13
  11.3 0.2 convolution_add_fusion
  11.6 0.2 convolution_add_fusion.1
  11.8 0.8 pad_maximum_fusion
  12.5 0.0 copy-start.9
  12.5 0.0 reduce-scatter.2.cloned.1.call-update
  12.6 0.0 copy-start.8
  12.6 0.0 all-gather.2.cloned.1.call-start
  12.6 0.0 copy-start.10
  12.6 0.0 copy-start.11
  12.7 126.3 %reduce-scatter.2.cloned.1.call-done = f32[8,768]{1,0:T(8,128)} async-done(((f32[128,768]{1,0:T(8,128)}), f32[8,768]{1,0:T(8,128)}) %reduce-scatter.2.cloned.1.call-update) | async-done | bytes 24592 | tf_op jit(solution)/shard_map/reduce_scatter | solution.py:56
  138.9 0.0 copy-done.9
  138.9 0.0 copy-done.8
  138.9 1.9 multiply_reduce_fusion
  140.9 0.0 copy-done.10
  140.9 0.0 copy-done.11
  140.9 1.9 multiply_reduce_fusion.1
  142.8 40.4 %all-reduce = (f32[]{:T(128)}, f32[]{:T(128)}) all-reduce(f32[]{:T(128)} %get-tuple-element.20, f32[]{:T(128)} %get-tuple-element.16), channel_id=1, replica_groups=mesh['fs'=4,'rep'=4,'tp'=2] {'fs','rep','tp'}, use_global_device_ids=true, to_apply=%region_2.0 | all-reduce | flops 2 | bytes 16 | tf_op jit(solution)/shard_map/psum | solution.py:85
  183.9 0.0 copy-start.6
  183.9 40.3 %all_gather.9 = f32[128,512]{1,0:T(8,128)S(1)} all-gather(f32[8,512]{1,0:T(8,128)S(1)} %get-tuple-element.17), channel_id=1, replica_groups=mesh['fs'=4,'rep'=4,'tp'=2] {'fs','rep'}, dimensions={0}, use_global_device_ids=true | all-gather | bytes 278528 | tf_op jit(solution)/shard_map/all_gather | solution.py:83
  224.2 0.0 copy-done.6
  224.2 1.0 fusion.7
  225.2 0.0 all-gather.2.cloned.1.call-update
  225.2 0.7 stack.2
  225.9 0.0 copy-start.7
  225.9 3.6 %all-to-all-start = ((f32[16,8,256]{2,1,0:T(8,128)}), f32[16,8,256]{2,1,0:T(8,128)S(1)}, u32[]{:S(2)}, u32[]{:S(2)}) async-start(f32[16,8,256]{2,1,0:T(8,128)} %stack.2), calls=%async_computation.1 | async-start | bytes 262144 | tf_op jit(solution)/shard_map/all_to_all | solution.py:78
  230.2 7.3 %all-to-all-done = f32[16,8,256]{2,1,0:T(8,128)S(1)} async-done(((f32[16,8,256]{2,1,0:T(8,128)}), f32[16,8,256]{2,1,0:T(8,128)S(1)}, u32[]{:S(2)}, u32[]{:S(2)}) %all-to-all-start) | async-done | bytes 131104 | tf_op jit(solution)/shard_map/all_to_all | solution.py:78
  237.5 0.0 copy-done.7
  237.5 0.8 fusion.8
  238.3 41.1 %all_gather.10 = bf16[1024,256]{1,0:T(8,128)(2,1)S(1)} all-gather(bf16[64,256]{1,0:T(8,128)(2,1)S(1)} %get-tuple-element.14), channel_id=1, replica_groups=mesh['fs'=4,'rep'=4,'tp'=2] {'fs','rep'}, dimensions={0}, use_global_device_ids=true | all-gather | bytes 557056 | tf_op jit(solution)/shard_map/all_gather | solution.py:104
  279.4 0.0 all-gather.2.cloned.1.call-done
  279.4 0.8 copy.23
  280.2 0.6 copy-done.1
  280.8 1.0 copy.24
  (1 shorter events, 0.0 us)
Async XLA Ops:
  7.2 1.0 copy-start
  7.2 2.2 copy-start.3
  7.2 131.7 %reduce-scatter.2.cloned.1.call-start = ((), (), s32[]{:S(2)}) async-start(), calls=%async_computation.2 | async-start | bytes 417792 | tf_op jit(solution)/shard_map/reduce_scatter | solution.py:56
  8.1 1.5 copy-start.4
  9.3 1.0 copy-start.2
  10.3 0.8 copy-start.5
  12.5 126.4 %copy-start.9 = (f32[8,512]{1,0:T(8,128)S(1)}, f32[8,512]{1,0:T(8,128)}, u32[]{:S(2)}) copy-start(f32[8,512]{1,0:T(8,128)} %param.20) | copy-start | bytes 49156
  12.6 126.4 %copy-start.8 = (f32[8,512]{1,0:T(8,128)S(1)}, f32[8,512]{1,0:T(8,128)}, u32[]{:S(2)}) copy-start(f32[8,512]{1,0:T(8,128)} %param.21) | copy-start | bytes 49156
  12.6 266.8 %all-gather.2.cloned.1.call-start = ((), (), s32[]{:S(2)}) async-start(), calls=%async_computation.3 | async-start | bytes 1114112 | tf_op jit(solution)/shard_map/all_gather | solution.py:105
  12.6 128.2 %copy-start.10 = (f32[8,256]{1,0:T(8,128)S(1)}, f32[8,256]{1,0:T(8,128)}, u32[]{:S(2)}) copy-start(f32[8,256]{1,0:T(8,128)} %param.19) | copy-start | bytes 24580
  12.6 128.2 %copy-start.11 = (f32[8,256]{1,0:T(8,128)S(1)}, f32[8,256]{1,0:T(8,128)}, u32[]{:S(2)}) copy-start(f32[8,256]{1,0:T(8,128)} %param.18) | copy-start | bytes 24580
  183.9 40.4 %copy-start.6 = (f32[64,512]{1,0:T(8,128)S(1)}, f32[64,512]{1,0:T(8,128)}, u32[]{:S(2)}) copy-start(f32[64,512]{1,0:T(8,128)} %param.17) | copy-start | bytes 393220
  225.9 11.6 %copy-start.7 = (f32[64,256]{1,0:T(8,128)S(1)}, f32[64,256]{1,0:T(8,128)}, u32[]{:S(2)}) copy-start(f32[64,256]{1,0:T(8,128)} %param.16) | copy-start | bytes 196612
  225.9 11.6 %all-to-all-start = ((f32[16,8,256]{2,1,0:T(8,128)}), f32[16,8,256]{2,1,0:T(8,128)S(1)}, u32[]{:S(2)}, u32[]{:S(2)}) async-start(f32[16,8,256]{2,1,0:T(8,128)} %stack.2), calls=%async_computation.1 | async-start | bytes 262144 | tf_op jit(solution)/shard_map/all_to_all | solution.py:78
  279.4 1.4 copy-start.1
Sparse Core Ops, SparseCore 0:
  13.2 125.6 reduce-scatter.1
  225.3 52.6 all-gather.1

commit v2 on v0

--- a/solution.py
+++ b/solution.py
@@ -78,7 +78,8 @@
         lax.all_gather(value_dir, ("fs", "rep"), axis=0, tiled=True),
     )
     query_squares, value_squares = lax.psum(
-        (jnp.sum(query_dir * query_dir), jnp.sum(value_dir * value_dir)), ("fs", "rep", "tp")
+        lax.psum((jnp.sum(query_dir * query_dir), jnp.sum(value_dir * value_dir)), ("rep", "tp")),
+        "fs",
     )
     tp_count = lax.axis_size("tp")
     query_update, query_weight_new, query_half = finish(

time: 314 us -> 294 us (0.936)
  blocking collectives: 159 us -> 138 us
    psum x1, blocking collectives: 40.4 us -> 12.5 us  [body(): lax.psum((jnp.sum(query_dir * query_dir), jnp.sum(value_dir * value_dir))...]
    psum x0 -> x1, blocking collectives: none -> 11.3 us  [body(): lax.psum(lax.psum((jnp.sum(query_dir * query_dir), jnp.sum(value_dir * va...]
    all_gather x1, blocking collectives: 40.3 us -> 37 us  [body(): lax.all_gather(value_dir, ('fs', 'rep'), axis=0, tiled=True)]
where the time goes in v2:
time: 294 us; the launch traced here: 293 us
  blocking collectives  138 us (47%)
  waiting for transfers between devices  126 us (43%)
  between operations  15.6 us (5%)
  local copies, waits for them, and re-layouts  4.65 us (2%)
  other arithmetic  4.61 us (2%)
  matrix products  4.03 us (1%)
    reduce_scatter x1, waiting for transfers between devices, body(): lax.psum_scatter(jnp.concatenate([parts_product(query_high, query_low, qu...  126 us
    all_gather x1, blocking collectives, body(): lax.all_gather(query_half, ('fs', 'rep'), axis=0, tiled=True)  38.8 us
    all_gather x1, blocking collectives, body(): lax.all_gather(query_dir, ('fs', 'rep'), axis=0, tiled=True)  38.4 us
    all_gather x1, blocking collectives, body(): lax.all_gather(value_dir, ('fs', 'rep'), axis=0, tiled=True)  37 us
    psum x1, blocking collectives, body(): lax.psum((jnp.sum(query_dir * query_dir), jnp.sum(value_dir * value_dir))...  12.5 us
    psum x1, blocking collectives, body(): lax.psum(lax.psum((jnp.sum(query_dir * query_dir), jnp.sum(value_dir * va...  11.3 us
  transfers between devices with their start and end apart: 2, of which 1 were waited for; matrix products, arithmetic and copies ran while one was open for 0% of the time, Pallas kernels for 0%

profile of v2, /device:TPU:0, one launch (start us, length us, event | category | flops | bytes accessed | tf_op | source)
XLA Modules:
  0.0 293.2 jit_solution(6767087489298853209)
XLA Ops:
  7.2 0.0 copy-start
  7.2 0.0 copy-start.3
  7.2 0.0 reduce-scatter.2.cloned.1.call-start
  7.2 0.9 copy-done
  8.1 0.0 copy-start.4
  8.1 1.2 fusion.10
  9.3 0.0 copy-start.2
  9.4 0.0 copy-done.3
  9.4 0.2 fusion.13
  9.6 0.0 copy-done.4
  9.6 0.7 copy-done.2
  10.3 0.0 copy-start.5
  10.3 0.2 fusion.11
  10.5 0.6 copy-done.5
  11.1 0.2 fusion.12
  11.3 0.2 convolution_add_fusion
  11.6 0.2 convolution_add_fusion.1
  11.8 0.8 pad_maximum_fusion
  12.5 0.0 copy-start.9
  12.5 0.0 reduce-scatter.2.cloned.1.call-update
  12.6 0.0 copy-start.8
  12.6 0.0 all-gather.2.cloned.1.call-start
  12.6 0.0 copy-start.10
  12.6 0.0 copy-start.11
  12.7 126.3 %reduce-scatter.2.cloned.1.call-done = f32[8,768]{1,0:T(8,128)} async-done(((f32[128,768]{1,0:T(8,128)}), f32[8,768]{1,0:T(8,128)}) %reduce-scatter.2.cloned.1.call-update) | async-done | bytes 24592 | tf_op jit(solution)/shard_map/reduce_scatter | solution.py:56
  138.9 0.0 copy-done.9
  138.9 0.0 copy-done.8
  138.9 1.9 multiply_reduce_fusion
  140.9 0.0 copy-done.10
  140.9 0.0 copy-done.11
  140.9 1.9 multiply_reduce_fusion.1
  142.8 12.5 %all-reduce = (f32[]{:T(128)}, f32[]{:T(128)}) all-reduce(f32[]{:T(128)} %get-tuple-element.22, f32[]{:T(128)} %get-tuple-element.18), channel_id=1, replica_groups=mesh['fs'=4,'rep'=4,'tp'=2] {'rep','tp'}, use_global_device_ids=true, to_apply=%region_2.0 | all-reduce | flops 2 | bytes 16 | tf_op jit(solution)/shard_map/psum | solution.py:81
  155.2 11.3 %all-reduce.1 = (f32[]{:T(128)}, f32[]{:T(128)}) all-reduce(f32[]{:T(128)} %get-tuple-element.10, f32[]{:T(128)} %get-tuple-element.11), channel_id=1, replica_groups=mesh['fs'=4,'rep'=4,'tp'=2] {'fs'}, use_global_device_ids=true, to_apply=%region_3.0 | all-reduce | flops 2 | bytes 16 | tf_op jit(solution)/shard_map/psum | solution.py:80
  167.2 0.0 copy-start.6
  167.3 37.0 %all_gather.13 = f32[128,512]{1,0:T(8,128)S(1)} all-gather(f32[8,512]{1,0:T(8,128)S(1)} %get-tuple-element.19), channel_id=1, replica_groups=mesh['fs'=4,'rep'=4,'tp'=2] {'fs','rep'}, dimensions={0}, use_global_device_ids=true | all-gather | bytes 278528 | tf_op jit(solution)/shard_map/all_gather | solution.py:78
  204.3 0.0 copy-done.6
  204.3 1.0 fusion.6
  205.2 0.0 all-gather.2.cloned.1.call-update
  206.0 0.0 copy-start.7
  206.0 38.4 %all_gather.12 = f32[128,256]{1,0:T(8,128)S(1)} all-gather(f32[8,256]{1,0:T(8,128)S(1)} %get-tuple-element.23), channel_id=1, replica_groups=mesh['fs'=4,'rep'=4,'tp'=2] {'fs','rep'}, dimensions={0}, use_global_device_ids=true | all-gather | bytes 139264 | tf_op jit(solution)/shard_map/all_gather | solution.py:77
  244.4 0.0 copy-done.7
  244.4 0.8 fusion.7
  245.2 38.8 %all_gather.14 = bf16[1024,256]{1,0:T(8,128)(2,1)S(1)} all-gather(bf16[64,256]{1,0:T(8,128)(2,1)S(1)} %get-tuple-element.16), channel_id=1, replica_groups=mesh['fs'=4,'rep'=4,'tp'=2] {'fs','rep'}, dimensions={0}, use_global_device_ids=true | all-gather | bytes 557056 | tf_op jit(solution)/shard_map/all_gather | solution.py:100
  284.0 0.0 all-gather.2.cloned.1.call-done
  284.0 0.0 copy-start.1
  284.0 0.8 copy.23
  284.8 0.6 copy-done.1
  285.4 1.0 copy.24
Async XLA Ops:
  7.2 1.0 copy-start
  7.2 2.2 copy-start.3
  7.2 131.7 %reduce-scatter.2.cloned.1.call-start = ((), (), s32[]{:S(2)}) async-start(), calls=%async_computation.1 | async-start | bytes 417792 | tf_op jit(solution)/shard_map/reduce_scatter | solution.py:56
  8.1 1.5 copy-start.4
  9.3 1.0 copy-start.2
  10.3 0.8 copy-start.5
  12.5 126.4 %copy-start.9 = (f32[8,512]{1,0:T(8,128)S(1)}, f32[8,512]{1,0:T(8,128)}, u32[]{:S(2)}) copy-start(f32[8,512]{1,0:T(8,128)} %param.20) | copy-start | bytes 49156
  12.6 126.4 %copy-start.8 = (f32[8,512]{1,0:T(8,128)S(1)}, f32[8,512]{1,0:T(8,128)}, u32[]{:S(2)}) copy-start(f32[8,512]{1,0:T(8,128)} %param.21) | copy-start | bytes 49156
  12.6 271.4 %all-gather.2.cloned.1.call-start = ((), (), s32[]{:S(2)}) async-start(), calls=%async_computation.2 | async-start | bytes 1114112 | tf_op jit(solution)/shard_map/all_gather | solution.py:101
  12.6 128.2 %copy-start.10 = (f32[8,256]{1,0:T(8,128)S(1)}, f32[8,256]{1,0:T(8,128)}, u32[]{:S(2)}) copy-start(f32[8,256]{1,0:T(8,128)} %param.19) | copy-start | bytes 24580
  12.6 128.2 %copy-start.11 = (f32[8,256]{1,0:T(8,128)S(1)}, f32[8,256]{1,0:T(8,128)}, u32[]{:S(2)}) copy-start(f32[8,256]{1,0:T(8,128)} %param.18) | copy-start | bytes 24580
  167.2 37.0 %copy-start.6 = (f32[64,512]{1,0:T(8,128)S(1)}, f32[64,512]{1,0:T(8,128)}, u32[]{:S(2)}) copy-start(f32[64,512]{1,0:T(8,128)} %param.17) | copy-start | bytes 393220
  206.0 38.4 %copy-start.7 = (f32[64,256]{1,0:T(8,128)S(1)}, f32[64,256]{1,0:T(8,128)}, u32[]{:S(2)}) copy-start(f32[64,256]{1,0:T(8,128)} %param.16) | copy-start | bytes 196612
  284.0 1.4 copy-start.1
Sparse Core Ops, SparseCore 0:
  13.2 125.6 reduce-scatter.1
  205.4 54.4 all-gather.1
